TPU v7x, 512 devices: a whole 4x8x8 slice. The times are simulated.
512 devices in a mesh: sp: 64 (over z, y), tp: 8 (over x, core).
Axes of the slice: x: 4, y: 8, z: 8, core: 2. Of those that a mesh axis runs over, the one named last changes fastest.
Arguments:
- queries: bfloat16 [16384, 1024], P('sp', 'tp'), may hold values from -6 to 6
- keys: bfloat16 [16384, 256], P('sp'), may hold values from -6 to 6
- values: bfloat16 [16384, 256], P('sp'), may hold values from -6 to 6
- query_gain: float32 [128], replicated, may hold values from 1.4 to 5.5
- key_gain: float32 [128], replicated, may hold values from 1.4 to 5.5
- residual_in: bfloat16 [16384, 2048], P(('sp', 'tp')), may hold values from -6 to 6
- out_weight: bfloat16 [1024, 2048], P('tp'), may hold values from -0.1875 to 0.1875
- norm_gain: float32 [2048], replicated, may hold values from 0.1 to 1.9
- gate_weight: bfloat16 [2048, 3072], P('sp', 'tp'), may hold values from -0.125 to 0.125
- up_weight: bfloat16 [2048, 3072], P('sp', 'tp'), may hold values from -0.125 to 0.125
- down_weight: bfloat16 [3072, 2048], P('tp', 'sp'), may hold values from -0.109375 to 0.109375
Outputs:
- result: bfloat16 [16384, 2048], P(('sp', 'tp'))
All inputs are finite; a program needn't handle non-finite values.
Results may differ from a plain program's by a relative error of at most 0.017.
Values may be sent and summed in bfloat16 or wider, within the bound.
A program may use at most 64 MiB of HBM per device.

v0:
```python
import math
import jax
import jax.numpy as jnp
from jax import lax
from jax.sharding import Mesh
from jax.sharding import PartitionSpec as P

Q_HEADS = 8
KV_HEADS = 2
GRID_WIDTH = 64
SP = ("sp_0", "sp_1")
SP_TP = ("sp_0", "sp_1", "tp")
EPS = 1e-06
ROPE_BASE = 10000.0


def side_by_side(arrays, axis, dim, along):
    widths = [a.shape[along] for a in arrays]
    both = jnp.concatenate(arrays, axis=along)
    result = lax.all_gather(both, axis, axis=dim, tiled=True)
    return tuple(jnp.split(result, [sum(widths[:k]) for k in range(1, len(widths))], axis=along))


def in_order(parts, dim):
    parts = jnp.moveaxis(parts, 0, dim)
    dims = parts.shape
    return parts.reshape(*dims[:dim], dims[dim] * dims[dim + 1], *dims[dim + 2 :])


def stacked_from(value, axes, turns):
    parts = value[None]
    for k in turns:
        parts = lax.all_gather(parts, axes[k], axis=0, tiled=True)
    block = [lax.axis_size(axes[k]) for k in reversed(turns)]
    parts = parts.reshape(*block, *value.shape)
    turned = sorted(range(len(turns)), key=lambda place: turns[len(turns) - 1 - place])
    return parts.transpose(*turned, *range(len(turns), parts.ndim)).reshape(-1, *value.shape)


def whole_of(value, axes, turns, dim):
    return in_order(stacked_from(value, axes, turns), dim)


def split_up(value, dim, size):
    before, after = (value.shape[:dim], value.shape[dim + 1 :])
    return jnp.moveaxis(value.reshape(*before, size, -1, *after), dim, 0)


def sent_and_summed(value, axis, dim):
    parts = split_up(value, dim, lax.axis_size(axis))
    arrived = lax.all_to_all(parts, axis, split_axis=0, concat_axis=0, tiled=True)
    return arrived.astype(jnp.float32).sum(axis=0)


def sent_to_all(value, axis):
    size = lax.axis_size(axis)
    return lax.all_to_all(
        jnp.broadcast_to(value[None], (size, *value.shape)), axis, 0, 0, tiled=True
    )


def gather_directly(value, axis, dim):
    return in_order(sent_to_all(value, axis), dim)


def normalize(wide_values, gain):
    wide = wide_values.astype(jnp.float32)
    return wide * lax.rsqrt(jnp.mean(wide * wide, axis=-1, keepdims=True) + EPS) * gain


def rotate_pair(segment, angles):
    half_size = segment.shape[-1] // 2
    first = segment[..., :half_size]
    second = segment[..., half_size:]
    cosine = jnp.cos(angles)[:, None, :]
    sine_part = jnp.sin(angles)[:, None, :]
    return jnp.concatenate(
        [first * cosine - second * sine_part, second * cosine + first * sine_part], axis=-1
    )


def grid_rotary(head_rows, positions):
    head_size = head_rows.shape[-1]
    half_size = head_size // 2
    quarter = head_size // 4
    inverse = ROPE_BASE ** (-jnp.arange(quarter, dtype=jnp.float32) * 2.0 / half_size)
    row_angles = (positions // GRID_WIDTH).astype(jnp.float32)[:, None] * inverse
    col_angles = (positions % GRID_WIDTH).astype(jnp.float32)[:, None] * inverse
    return jnp.concatenate(
        [
            rotate_pair(head_rows[..., :half_size], row_angles),
            rotate_pair(head_rows[..., half_size:], col_angles),
        ],
        axis=-1,
    )


def gated(gate_part, lifted):
    return (jax.nn.silu(gate_part) * lifted).astype(jnp.bfloat16)


def local(
    queries,
    keys,
    values,
    query_gain,
    key_gain,
    residual_in,
    out_weight,
    norm_gain,
    gate_weight,
    up_weight,
    down_weight,
):
    tok_rows = queries.shape[0]
    head_size = query_gain.shape[0]
    local_heads = queries.shape[1] // head_size
    tp_index = lax.axis_index("tp")
    gate_full, up_full = side_by_side((gate_weight, up_weight), SP, 0, 1)
    down_full = whole_of(down_weight, SP, (0, 1), 1)
    positions = lax.axis_index(SP) * tok_rows + jnp.arange(tok_rows, dtype=jnp.int32)
    key_head = tp_index * local_heads // (Q_HEADS // KV_HEADS)
    own_keys = lax.dynamic_slice_in_dim(keys, key_head * head_size, head_size, 1)
    own_values = lax.dynamic_slice_in_dim(values, key_head * head_size, head_size, 1)
    turned_keys = grid_rotary(
        normalize(own_keys.reshape(tok_rows, 1, head_size), key_gain), positions
    )
    turned_keys = turned_keys.reshape(tok_rows, head_size).astype(jnp.bfloat16)
    turned_queries = grid_rotary(
        normalize(queries.reshape(tok_rows, local_heads, head_size), query_gain), positions
    )
    turned_queries = turned_queries.reshape(tok_rows * local_heads, head_size).astype(jnp.bfloat16)
    score_scale = head_size ** (-0.5)

    def attend_block(running, block_pair):
        peak_score, weight_total, weighted = running
        block_keys, block_values = block_pair
        scores = (
            lax.dot_general(
                turned_queries,
                block_keys,
                (((1,), (1,)), ((), ())),
                preferred_element_type=jnp.float32,
            )
            * score_scale
        )
        new_peak = jnp.maximum(peak_score, jnp.max(scores, axis=1))
        factor = jnp.exp(peak_score - new_peak)
        raw = jnp.exp(scores - new_peak[:, None])
        weight_total = weight_total * factor + jnp.sum(raw, axis=1)
        weighted = weighted * factor[:, None] + jnp.dot(
            raw.astype(jnp.bfloat16), block_values, preferred_element_type=jnp.float32
        )
        return ((new_peak, weight_total, weighted), None)

    row_count = tok_rows * local_heads
    start_carry = (
        jnp.full((row_count,), -1e30, jnp.float32),
        jnp.zeros((row_count,), jnp.float32),
        jnp.zeros((row_count, head_size), jnp.float32),
    )
    piece_keys, piece_values = side_by_side((turned_keys, own_values), SP, 0, 1)
    span = math.gcd(piece_keys.shape[0], 512)
    blocks = piece_keys.shape[0] // span
    stacked = (
        piece_keys.reshape(blocks, span, head_size),
        piece_values.reshape(blocks, span, head_size),
    )
    updated, unused = lax.scan(attend_block, start_carry, stacked)
    peak_score, weight_total, weighted = updated
    attended = (weighted / weight_total[:, None]).astype(jnp.bfloat16)
    attention_out = sent_and_summed(
        jnp.dot(attended, out_weight, preferred_element_type=jnp.float32).astype(jnp.bfloat16),
        "tp",
        0,
    )
    middle = (residual_in.astype(jnp.float32) + attention_out).astype(jnp.bfloat16)
    normed = gather_directly(normalize(middle, norm_gain).astype(jnp.bfloat16), "tp", 0)
    hidden = gated(
        jnp.dot(normed, gate_full, preferred_element_type=jnp.float32),
        jnp.dot(normed, up_full, preferred_element_type=jnp.float32),
    )
    partials = jnp.dot(hidden, down_full, preferred_element_type=jnp.float32)
    mixer_out = sent_and_summed(partials.astype(jnp.bfloat16), "tp", 0)
    return (middle.astype(jnp.float32) + mixer_out).astype(jnp.bfloat16)


def solution(mesh):
    finer = Mesh(mesh.devices.reshape(8, 8, mesh.shape["tp"]), ("sp_0", "sp_1", "tp"))
    in_specs = (
        P(SP, "tp"),
        P(SP, None),
        P(SP, None),
        P(),
        P(),
        P(SP_TP, None),
        P("tp", None),
        P(),
        P(SP, "tp"),
        P(SP, "tp"),
        P("tp", SP),
    )
    out_specs = P(SP_TP, None)
    return jax.shard_map(local, mesh=finer, in_specs=in_specs, out_specs=out_specs, check_vma=False)
```

profile of v0, /device:TPU:1, one launch (start us, length us, event | category | flops | bytes accessed | tf_op | source)
XLA Modules:
  0.0 299.4 jit_solution(13438292741110055341)
XLA Ops:
  11.4 26.1 %all-gather = bf16[3072,32]{0,1:T(8,128)(2,1)S(1)} all-gather(bf16[384,32]{0,1:T(8,128)(2,1)} %param.23), channel_id=2, replica_groups=mesh['sp_0'=8,'sp_1'=8,'tp'=8] {'sp_0'}, dimensions={0}, use_global_device_ids=true | all-gather | bytes 221184 | tf_op jit(solution)/shard_map/all_gather | solution.py:33
  38.2 1.4 pad_maximum_fusion.1
  39.8 80.1 %all-gather.5.cloned.1.call-done = bf16[16384,256]{0,1:T(8,128)(2,1)} async-done(((bf16[256,256]{0,1:T(8,128)(2,1)}), bf16[16384,256]{0,1:T(8,128)(2,1)}) %all-gather.5.cloned.1.call-update) | async-done | bytes 8388624 | tf_op jit(solution)/shard_map/all_gather | solution.py:20
  119.9 5.8 %fusion.78 = (bf16[16384,128]{0,1:T(8,128)(2,1)}, bf16[16384,128]{0,1:T(8,128)(2,1)}) fusion(bf16[16384,256]{0,1:T(8,128)(2,1)} %all-gather.5.cloned.1.call-done), kind=kLoop, calls=%fused_computation.112 | loop fusion | bytes 16777216 | tf_op jit(solution)/shard_map/split | solution.py:21
  125.7 6.4 %copy.23 = bf16[16384,128]{1,0:T(8,128)(2,1)} copy(bf16[16384,128]{0,1:T(8,128)(2,1)} %get-tuple-element.97) | data formatting | bytes 8388608
  132.0 6.4 %copy.24 = bf16[16384,128]{1,0:T(8,128)(2,1)} copy(bf16[16384,128]{0,1:T(8,128)(2,1)} %get-tuple-element.96) | data formatting | bytes 8388608
  138.4 81.8 %while.15 = (s32[]{:T(128)}, f32[256]{0:T(256)S(1)}, f32[256]{0:T(256)S(1)}, f32[256,128]{1,0:T(8,128)S(1)}, bf16[32,512,128]{2,1,0:T(8,128)(2,1)}, /*index=5*/b...) while((s32[]{:T(128)}, f32[256]{0:T(256)S(1)}, ...), condition=%wide.region_5.6_spmd.clone, body=%wide.region_2.5_spmd.clone.sunk | while | flops 67994880 | bytes 2180201 | solution.py:169
  139.8 1.2 convolution_add_fusion.2
  142.3 1.2 convolution_add_fusion.2
  143.5 1.2 fusion.94
  144.9 1.2 convolution_add_fusion.2
  147.4 1.2 convolution_add_fusion.2
  148.7 1.2 fusion.94
  150.0 1.2 convolution_add_fusion.2
  151.2 1.2 fusion.94
  152.5 1.2 convolution_add_fusion.2
  153.8 1.2 fusion.94
  155.1 1.2 convolution_add_fusion.2
  156.3 1.2 fusion.94
  157.7 1.2 convolution_add_fusion.2
  160.2 1.2 convolution_add_fusion.2
  161.4 1.2 fusion.94
  162.8 1.2 convolution_add_fusion.2
  165.3 1.2 convolution_add_fusion.2
  166.6 1.2 fusion.94
  167.9 1.2 convolution_add_fusion.2
  170.4 1.2 convolution_add_fusion.2
  171.7 1.2 fusion.94
  173.0 1.2 convolution_add_fusion.2
  175.6 1.2 convolution_add_fusion.2
  176.8 1.2 fusion.94
  178.1 1.2 convolution_add_fusion.2
  180.7 1.2 convolution_add_fusion.2
  183.2 1.2 convolution_add_fusion.2
  184.4 1.2 fusion.94
  185.8 1.2 convolution_add_fusion.2
  188.3 1.2 convolution_add_fusion.2
  189.5 1.2 fusion.94
  190.9 1.2 convolution_add_fusion.2
  193.4 1.2 convolution_add_fusion.2
  194.7 1.2 fusion.94
  196.0 1.2 convolution_add_fusion.2
  197.2 1.2 fusion.94
  198.6 1.2 convolution_add_fusion.2
  201.1 1.2 convolution_add_fusion.2
  202.3 1.2 fusion.94
  203.7 1.2 convolution_add_fusion.2
  204.9 1.2 fusion.94
  206.2 1.2 convolution_add_fusion.2
  207.4 1.2 fusion.94
  208.8 1.2 convolution_add_fusion.2
  211.3 1.2 convolution_add_fusion.2
  212.6 1.2 fusion.94
  213.9 1.2 convolution_add_fusion.2
  216.4 1.2 convolution_add_fusion.2
  217.7 1.2 fusion.94
  219.0 1.2 convolution_add_fusion.2
  220.7 24.3 %all_to_all.15 = bf16[8,32,2048]{2,1,0:T(8,128)(2,1)S(1)} all-to-all(bf16[8,32,2048]{2,1,0:T(8,128)(2,1)S(1)} %bitcast.46), channel_id=1, replica_groups=mesh['sp_0'=8,'sp_1'=8,'tp'=8] {'tp'}, dimensions={0} | all-to-all | bytes 2097152 | tf_op jit(solution)/shard_map/all_to_all | solution.py:51
  246.6 4.5 %all-to-all-start.1 = ((bf16[8,32,2048]{2,1,0:T(8,128)(2,1)}), bf16[8,32,2048]{2,1,0:T(8,128)(2,1)S(1)}, u32[]{:S(2)}, u32[]{:S(2)}) async-start(bf16[8,32,2048]{2,1,0:T(8,128)(2,1)} %broadcast_in_dim.13), calls=%async_computation.1 | async-start | bytes 2097152 | tf_op jit(solution)/shard_map/all_to_all | solution.py:57
  251.1 2.3 copy.22
  253.4 12.6 %all-to-all-done.1 = bf16[8,32,2048]{2,1,0:T(8,128)(2,1)S(1)} async-done(((bf16[8,32,2048]{2,1,0:T(8,128)(2,1)}), bf16[8,32,2048]{2,1,0:T(8,128)(2,1)S(1)}, u32[]{:S(2)}, u32[]{:S(2)}) %all-to-all-start.1) | async-done | bytes 1048608 | tf_op jit(solution)/shard_map/all_to_all | solution.py:57
  266.1 2.9 fusion.14
  268.9 3.8 %convolution_convert_fusion = bf16[256,2048]{1,0:T(8,128)(2,1)} fusion(bf16[384,2048]{0,1:T(8,128)(2,1)S(1)} %bitcast.48, bf16[256,2048]{1,0:T(8,128)(2,1)S(1)} %bitcast.50, bf16[2048,768]{1,0:T(8,128)(2,1)} %all-gather.7.cloned.1.call-done, f32[256,384]{1,0:T(8,128)} %fusion.14), kind=kOutput, calls=%fused_computation.18 | convolution fusion | flops 806420480 | bytes 5636096 | tf_op jit(solution)/shard_map/dot_general | solution.py:183
  272.7 19.4 %all_to_all.16 = bf16[8,32,2048]{2,1,0:T(8,128)(2,1)S(1)} all-to-all(bf16[8,32,2048]{2,1,0:T(8,128)(2,1)} %bitcast.51), channel_id=1, replica_groups=mesh['sp_0'=8,'sp_1'=8,'tp'=8] {'tp'}, dimensions={0} | all-to-all | bytes 2097152 | tf_op jit(solution)/shard_map/all_to_all | solution.py:51
  (185 shorter events, 29.6 us)
Async XLA Ops:
  6.5 213.7 %copy-start = (bf16[128,2048]{1,0:T(8,128)(2,1)S(1)}, bf16[128,2048]{1,0:T(8,128)(2,1)}, u32[]{:S(2)}) copy-start(bf16[128,2048]{1,0:T(8,128)(2,1)} %param.19) | copy-start | bytes 1572868
  6.5 113.3 %all-gather.5.cloned.1.call-start = ((), (), s32[]{:S(2)}) async-start(), calls=%async_computation.3 | async-start | bytes 8519680 | tf_op jit(solution)/shard_map/all_gather | solution.py:20
  11.3 239.7 %all-gather.9.cloned.1.call-start = ((), (), s32[]{:S(2)}) async-start(), calls=%async_computation.5 | async-start | bytes 1769472 | tf_op jit(solution)/shard_map/all_gather | solution.py:33
  38.2 215.2 %all-gather.7.cloned.1.call-start = ((), (), s32[]{:S(2)}) async-start(), calls=%async_computation.4 | async-start | bytes 3194880 | tf_op jit(solution)/shard_map/all_gather | solution.py:20
  220.2 25.0 %copy-start.1 = (bf16[32,2048]{1,0:T(8,128)(2,1)S(1)}, bf16[32,2048]{1,0:T(8,128)(2,1)}, u32[]{:S(2)}) copy-start(bf16[32,2048]{1,0:T(8,128)(2,1)} %param.18) | copy-start | bytes 393220
  220.2 25.1 %copy-start.2 = (f32[2048]{0:T(1024)S(1)}, f32[2048]{0:T(1024)}, u32[]{:S(2)}) copy-start(f32[2048]{0:T(1024)} %param.20) | copy-start | bytes 24580
  246.6 19.5 %all-to-all-start.1 = ((bf16[8,32,2048]{2,1,0:T(8,128)(2,1)}), bf16[8,32,2048]{2,1,0:T(8,128)(2,1)S(1)}, u32[]{:S(2)}, u32[]{:S(2)}) async-start(bf16[8,32,2048]{2,1,0:T(8,128)(2,1)} %broadcast_in_dim.13), calls=%async_computation.1 | async-start | bytes 2097152 | tf_op jit(solution)/shard_map/all_to_all | solution.py:57
Sparse Core Ops, SparseCore 0:
  11.5 108.3 all-gather.4
  122.0 38.1 all-gather.8
  163.1 85.2 all-gather.6
where the time goes:
time: 301 us; the launch traced here: 299 us
  waiting for transfers between devices  92.8 us (31%)
  matrix products  82.6 us (27%)
  blocking collectives  69.7 us (23%)
  local copies, waits for them, and re-layouts  25 us (8%)
  between operations  13.3 us (4%)
  other arithmetic  9.95 us (3%)
  starting transfers between devices  4.58 us (2%)
    all_gather x2, waiting for transfers between devices, side_by_side(): result = lax.all_gather(both, axis, axis=dim, tiled=True)  80.1 us
    all_to_all x2, blocking collectives, sent_and_summed(): lax.all_to_all(parts, axis, split_axis=0, concat_axis=0, tiled=True)  43.7 us
    dot_general x32, matrix products, attend_block(): jnp.dot(raw.astype(jnp.bfloat16), block_values, preferred_element_type=jn...  38.1 us
    dot_general x32, matrix products, attend_block(): lax.dot_general(turned_queries, block_keys, (((1,), (1,)), ((), ())), pre...  37.4 us
    all_gather x1, blocking collectives, stacked_from(): parts = lax.all_gather(parts, axes[k], axis=0, tiled=True)  26.1 us
    unnamed x13, local copies, waits for them, and re-layouts  14.7 us
    all_to_all x1, waiting for transfers between devices, sent_to_all(): lax.all_to_all(jnp.broadcast_to(value[None], (size, *value.shape)), axis,...  12.6 us
  transfers between devices with their start and end apart: 4, of which 2 were waited for; matrix products, arithmetic and copies ran while one was open for 35% of the time, Pallas kernels for 0%

commit v1 on v0

--- a/solution.py
+++ b/solution.py
@@ -30,7 +30,8 @@
 def stacked_from(value, axes, turns):
     parts = value[None]
     for k in turns:
-        parts = lax.all_gather(parts, axes[k], axis=0, tiled=True)
+        sent = jnp.stack([parts] * lax.axis_size(axes[k]))
+        parts = jnp.concatenate(lax.all_to_all(sent, axes[k], 0, 0), axis=0)
     block = [lax.axis_size(axes[k]) for k in reversed(turns)]
     parts = parts.reshape(*block, *value.shape)
     turned = sorted(range(len(turns)), key=lambda place: turns[len(turns) - 1 - place])

time: 301 us -> 348 us (1.16)
  waiting for transfers between devices: 92.8 us -> 148 us
  blocking collectives: 69.7 us -> 43.9 us
  starting transfers between devices: 4.58 us -> 19.3 us
    all_to_all x0 -> x2, waiting for transfers between devices: none -> 40 us  [stacked_from(): parts = jnp.concatenate(lax.all_to_all(sent, axes[k], 0, 0), axis=0)]
    all_gather x1 -> x0, blocking collectives: 26.1 us -> none  [stacked_from(): parts = lax.all_gather(parts, axes[k], axis=0, tiled=True)]
    all_to_all x0 -> x2, starting transfers between devices: none -> 15.2 us  [stacked_from(): parts = jnp.concatenate(lax.all_to_all(sent, axes[k], 0, 0), axis=0)]
    all_gather x2, waiting for transfers between devices: 80.1 us -> 94.6 us  [side_by_side(): result = lax.all_gather(both, axis, axis=dim, tiled=True)]
    unnamed x13 -> x14, local copies, waits for them, and re-layouts: 14.7 us -> 14.1 us
  transfers between devices with their start and end apart: 4 -> 5, of which waited for: 2 -> 3; matrix products, arithmetic and copies ran while one was open for 35% -> 31% of each run, Pallas kernels for 0% -> 0%
where the time goes in v1:
time: 348 us; the launch traced here: 346 us
  waiting for transfers between devices  148 us (43%)
  matrix products  83.6 us (24%)
  blocking collectives  43.9 us (13%)
  local copies, waits for them, and re-layouts  26.1 us (8%)
  starting transfers between devices  19.3 us (6%)
  between operations  13.6 us (4%)
  other arithmetic  9.94 us (3%)
    all_gather x2, waiting for transfers between devices, side_by_side(): result = lax.all_gather(both, axis, axis=dim, tiled=True)  94.6 us
    all_to_all x2, blocking collectives, sent_and_summed(): lax.all_to_all(parts, axis, split_axis=0, concat_axis=0, tiled=True)  43.9 us
    all_to_all x2, waiting for transfers between devices, stacked_from(): parts = jnp.concatenate(lax.all_to_all(sent, axes[k], 0, 0), axis=0)  40 us
    dot_general x32, matrix products, attend_block(): jnp.dot(raw.astype(jnp.bfloat16), block_values, preferred_element_type=jn...  38.1 us
    dot_general x32, matrix products, attend_block(): lax.dot_general(turned_queries, block_keys, (((1,), (1,)), ((), ())), pre...  37.4 us
    all_to_all x2, starting transfers between devices, stacked_from(): parts = jnp.concatenate(lax.all_to_all(sent, axes[k], 0, 0), axis=0)  15.2 us
    unnamed x14, local copies, waits for them, and re-layouts  14.1 us
    all_to_all x1, waiting for transfers between devices, sent_to_all(): lax.all_to_all(jnp.broadcast_to(value[None], (size, *value.shape)), axis,...  13.6 us
  transfers between devices with their start and end apart: 5, of which 3 were waited for; matrix products, arithmetic and copies ran while one was open for 31% of the time, Pallas kernels for 0%

profile of v1, /device:TPU:1, one launch (start us, length us, event | category | flops | bytes accessed | tf_op | source)
XLA Modules:
  0.0 346.0 jit_solution(15936420567894466784)
XLA Ops:
  11.3 1.4 stack.6
  12.8 10.9 %all-to-all-start.2 = ((bf16[8,1,384,32]{2,3,1,0:T(8,128)(2,1)}), bf16[8,1,384,32]{2,3,1,0:T(8,128)(2,1)S(1)}, u32[]{:S(2)}, u32[]{:S(2)}) async-start(bf16[8,1,384,32]{2,3,1,0:T(8,128)(2,1)} %stack.6), calls=%async_computation.2 | async-start | bytes 393216 | tf_op jit(solution)/shard_map/all_to_all | solution.py:34
  23.7 1.4 pad_maximum_fusion.1
  25.2 94.6 %all-gather.3.cloned.1.call-done = bf16[16384,256]{0,1:T(8,128)(2,1)} async-done(((bf16[256,256]{0,1:T(8,128)(2,1)}), bf16[16384,256]{0,1:T(8,128)(2,1)}) %all-gather.3.cloned.1.call-update) | async-done | bytes 8388624 | tf_op jit(solution)/shard_map/all_gather | solution.py:20
  119.9 5.8 %fusion.78 = (bf16[16384,128]{0,1:T(8,128)(2,1)}, bf16[16384,128]{0,1:T(8,128)(2,1)}) fusion(bf16[16384,256]{0,1:T(8,128)(2,1)} %all-gather.3.cloned.1.call-done), kind=kLoop, calls=%fused_computation.112 | loop fusion | bytes 16777216 | tf_op jit(solution)/shard_map/split | solution.py:21
  125.7 6.4 %copy.21 = bf16[16384,128]{1,0:T(8,128)(2,1)} copy(bf16[16384,128]{0,1:T(8,128)(2,1)} %get-tuple-element.97) | data formatting | bytes 8388608
  132.0 6.4 %copy.22 = bf16[16384,128]{1,0:T(8,128)(2,1)} copy(bf16[16384,128]{0,1:T(8,128)(2,1)} %get-tuple-element.96) | data formatting | bytes 8388608
  138.4 81.7 %while.15 = (s32[]{:T(128)}, f32[256]{0:T(256)S(1)}, f32[256]{0:T(256)S(1)}, f32[256,128]{1,0:T(8,128)S(1)}, bf16[32,512,128]{2,1,0:T(8,128)(2,1)}, /*index=5*/b...) while((s32[]{:T(128)}, f32[256]{0:T(256)S(1)}, ...), condition=%wide.region_5.6_spmd.clone, body=%wide.region_2.5_spmd.clone.sunk | while | flops 67994880 | bytes 2180201 | solution.py:170
  139.8 1.2 convolution_add_fusion.2
  141.0 1.2 fusion.94
  142.3 1.2 convolution_add_fusion.2
  143.5 1.2 fusion.94
  144.9 1.2 convolution_add_fusion.2
  146.1 1.2 fusion.94
  147.4 1.2 convolution_add_fusion.2
  148.6 1.2 fusion.94
  150.0 1.2 convolution_add_fusion.2
  151.2 1.2 fusion.94
  152.5 1.2 convolution_add_fusion.2
  153.8 1.2 fusion.94
  155.1 1.2 convolution_add_fusion.2
  156.3 1.2 fusion.94
  157.6 1.2 convolution_add_fusion.2
  158.9 1.2 fusion.94
  160.2 1.2 convolution_add_fusion.2
  162.7 1.2 convolution_add_fusion.2
  165.3 1.2 convolution_add_fusion.2
  167.8 1.2 convolution_add_fusion.2
  169.1 1.2 fusion.94
  170.4 1.2 convolution_add_fusion.2
  171.6 1.2 fusion.94
  172.9 1.2 convolution_add_fusion.2
  175.5 1.2 convolution_add_fusion.2
  178.0 1.2 convolution_add_fusion.2
  180.6 1.2 convolution_add_fusion.2
  181.8 1.2 fusion.94
  183.2 1.2 convolution_add_fusion.2
  185.7 1.2 convolution_add_fusion.2
  188.3 1.2 convolution_add_fusion.2
  190.8 1.2 convolution_add_fusion.2
  192.1 1.2 fusion.94
  193.4 1.2 convolution_add_fusion.2
  195.9 1.2 convolution_add_fusion.2
  197.2 1.2 fusion.94
  198.5 1.2 convolution_add_fusion.2
  201.1 1.2 convolution_add_fusion.2
  203.6 1.2 convolution_add_fusion.2
  206.2 1.2 convolution_add_fusion.2
  208.7 1.2 convolution_add_fusion.2
  211.3 1.2 convolution_add_fusion.2
  213.8 1.2 convolution_add_fusion.2
  216.4 1.2 convolution_add_fusion.2
  218.9 1.2 convolution_add_fusion.2
  220.1 1.5 convolution_convert_fusion.1
  221.6 24.5 %all_to_all.25 = bf16[8,32,2048]{2,1,0:T(8,128)(2,1)S(1)} all-to-all(bf16[8,32,2048]{2,1,0:T(8,128)(2,1)} %bitcast.42), channel_id=1, replica_groups=mesh['sp_0'=8,'sp_1'=8,'tp'=8] {'tp'}, dimensions={0} | all-to-all | bytes 2097152 | tf_op jit(solution)/shard_map/all_to_all | solution.py:52
  246.1 1.3 stack.7
  247.5 4.4 %all-to-all-start.3 = ((bf16[8,8,384,32]{2,3,1,0:T(8,128)(2,1)}), bf16[8,8,384,32]{2,3,1,0:T(8,128)(2,1)S(1)}, u32[]{:S(2)}, u32[]{:S(2)}) async-start(bf16[8,8,384,32]{2,3,1,0:T(8,128)(2,1)} %stack.7), calls=%async_computation.3 | async-start | bytes 3145728 | tf_op jit(solution)/shard_map/all_to_all | solution.py:34
  252.3 40.0 %all-to-all-done.3 = bf16[8,8,384,32]{2,3,1,0:T(8,128)(2,1)S(1)} async-done(((bf16[8,8,384,32]{2,3,1,0:T(8,128)(2,1)}), bf16[8,8,384,32]{2,3,1,0:T(8,128)(2,1)S(1)}, u32[]{:S(2)}, u32[]{:S(2)}) %all-to-all-start.3) | async-done | bytes 1572896 | tf_op jit(solution)/shard_map/all_to_all | solution.py:34
  293.4 4.0 %all-to-all-start.1 = ((bf16[8,32,2048]{2,1,0:T(8,128)(2,1)}), bf16[8,32,2048]{2,1,0:T(8,128)(2,1)S(1)}, u32[]{:S(2)}, u32[]{:S(2)}) async-start(bf16[8,32,2048]{2,1,0:T(8,128)(2,1)} %broadcast_in_dim.11), calls=%async_computation.1 | async-start | bytes 2097152 | tf_op jit(solution)/shard_map/all_to_all | solution.py:58
  297.4 1.4 copy.20
  298.7 13.6 %all-to-all-done.1 = bf16[8,32,2048]{2,1,0:T(8,128)(2,1)S(1)} async-done(((bf16[8,32,2048]{2,1,0:T(8,128)(2,1)}), bf16[8,32,2048]{2,1,0:T(8,128)(2,1)S(1)}, u32[]{:S(2)}, u32[]{:S(2)}) %all-to-all-start.1) | async-done | bytes 1048608 | tf_op jit(solution)/shard_map/all_to_all | solution.py:58
  312.4 2.9 fusion.14
  315.2 3.8 %convolution_convert_fusion = bf16[256,2048]{1,0:T(8,128)(2,1)} fusion(bf16[384,2048]{0,1:T(8,128)(2,1)S(1)} %bitcast.43, bf16[256,2048]{1,0:T(8,128)(2,1)S(1)} %bitcast.45, bf16[2048,768]{1,0:T(8,128)(2,1)} %all-gather.5.cloned.1.call-done, f32[256,384]{1,0:T(8,128)} %fusion.14), kind=kOutput, calls=%fused_computation.18 | convolution fusion | flops 806420480 | bytes 5636096 | tf_op jit(solution)/shard_map/dot_general | solution.py:184
  319.0 19.4 %all_to_all.26 = bf16[8,32,2048]{2,1,0:T(8,128)(2,1)S(1)} all-to-all(bf16[8,32,2048]{2,1,0:T(8,128)(2,1)} %bitcast.46), channel_id=1, replica_groups=mesh['sp_0'=8,'sp_1'=8,'tp'=8] {'tp'}, dimensions={0} | all-to-all | bytes 2097152 | tf_op jit(solution)/shard_map/all_to_all | solution.py:52
  (188 shorter events, 34.2 us)
Async XLA Ops:
  6.5 213.6 %copy-start = (bf16[128,2048]{1,0:T(8,128)(2,1)S(1)}, bf16[128,2048]{1,0:T(8,128)(2,1)}, u32[]{:S(2)}) copy-start(bf16[128,2048]{1,0:T(8,128)(2,1)} %param.19) | copy-start | bytes 1572868
  6.5 113.3 %all-gather.3.cloned.1.call-start = ((), (), s32[]{:S(2)}) async-start(), calls=%async_computation.5 | async-start | bytes 8519680 | tf_op jit(solution)/shard_map/all_gather | solution.py:20
  12.8 208.8 %all-to-all-start.2 = ((bf16[8,1,384,32]{2,3,1,0:T(8,128)(2,1)}), bf16[8,1,384,32]{2,3,1,0:T(8,128)(2,1)S(1)}, u32[]{:S(2)}, u32[]{:S(2)}) async-start(bf16[8,1,384,32]{2,3,1,0:T(8,128)(2,1)} %stack.6), calls=%async_computation.2 | async-start | bytes 393216 | tf_op jit(solution)/shard_map/all_to_all | solution.py:34
  23.6 275.1 %all-gather.5.cloned.1.call-start = ((), (), s32[]{:S(2)}) async-start(), calls=%async_computation.6 | async-start | bytes 3194880 | tf_op jit(solution)/shard_map/all_gather | solution.py:20
  246.1 5.9 %copy-start.2 = (bf16[32,2048]{1,0:T(8,128)(2,1)S(1)}, bf16[32,2048]{1,0:T(8,128)(2,1)}, u32[]{:S(2)}) copy-start(bf16[32,2048]{1,0:T(8,128)(2,1)} %param.18) | copy-start | bytes 393220
  246.1 6.1 %copy-start.3 = (f32[2048]{0:T(1024)S(1)}, f32[2048]{0:T(1024)}, u32[]{:S(2)}) copy-start(f32[2048]{0:T(1024)} %param.20) | copy-start | bytes 24580
  247.5 44.8 %all-to-all-start.3 = ((bf16[8,8,384,32]{2,3,1,0:T(8,128)(2,1)}), bf16[8,8,384,32]{2,3,1,0:T(8,128)(2,1)S(1)}, u32[]{:S(2)}, u32[]{:S(2)}) async-start(bf16[8,8,384,32]{2,3,1,0:T(8,128)(2,1)} %stack.7), calls=%async_computation.3 | async-start | bytes 3145728 | tf_op jit(solution)/shard_map/all_to_all | solution.py:34
  293.4 19.0 %all-to-all-start.1 = ((bf16[8,32,2048]{2,1,0:T(8,128)(2,1)}), bf16[8,32,2048]{2,1,0:T(8,128)(2,1)S(1)}, u32[]{:S(2)}, u32[]{:S(2)}) async-start(bf16[8,32,2048]{2,1,0:T(8,128)(2,1)} %broadcast_in_dim.11), calls=%async_computation.1 | async-start | bytes 2097152 | tf_op jit(solution)/shard_map/all_to_all | solution.py:58
  298.7 16.5 %copy-start.1 = (bf16[8,8,384,32]{2,3,0,1:T(8,128)(2,1)S(1)}, bf16[8,8,384,32]{2,3,0,1:T(8,128)(2,1)}, u32[]{:S(2)}) copy-start(bf16[8,8,384,32]{2,3,0,1:T(8,128)(2,1)} %copy.20) | copy-start | bytes 4718596
Sparse Core Ops, SparseCore 0:
  11.5 108.3 all-gather.2
  122.9 82.2 all-gather.4
